TPU v7x, 32 devices: a whole 2x2x4 slice. The times are simulated.
32 devices in a mesh: ra: 8 (over z, y), cb: 4 (over x, core).
Axes of the slice: x: 2, y: 2, z: 4, core: 2. Of those that a mesh axis runs over, the one named last changes fastest.
Arguments:
- stream: bfloat16 [64, 1024], P(None, 'ra'), may hold values from -24 to 24, as said below
- gain_first: float32 [1024], P('ra'), may hold values from 0.5 to 1.5
- up_first: float32 [1024, 4096], P('ra', 'cb'), may hold values from -0.1875 to 0.1875
- down_first: float32 [4096, 1024], P('cb', 'ra'), may hold values from -0.09375 to 0.09375
- gain_second: float32 [1024], P('ra'), may hold values from 0.5 to 1.5
- up_second: float32 [1024, 4096], P('ra', 'cb'), may hold values from -0.1875 to 0.1875
- down_second: float32 [4096, 1024], P('cb', 'ra'), may hold values from -0.09375 to 0.09375
Outputs:
- read: bfloat16 [64, 1024], P(None, 'ra')
Inputs may be any that keep to these rules, and one draw needn't show every extreme that they name: stream is of order one, and in each token one aligned block of 128 features is four times larger than the rest.
All inputs are finite; a program needn't handle non-finite values.
Results may differ from a plain program's by a relative error of at most 0.025.
Values may be sent and summed in bfloat16 or wider, within the bound.
A program may use at most 64 MiB of HBM per device.

v0:
```python
import jax
import jax.numpy as jnp
from jax import lax
from jax.sharding import PartitionSpec as P

D = 1024
EPS = 1e-06
RESIDUAL = 0.25


def sublayer(stream, norm_gain, w_up, w_down):
    floated = stream.astype(jnp.float32)
    own_squares = jnp.sum(floated * floated, axis=1, keepdims=True)
    squares = lax.psum(own_squares, "ra")
    factor = lax.rsqrt(squares / D + EPS)
    normed = (floated * factor * norm_gain.astype(jnp.float32)[None, :]).astype(jnp.bfloat16)
    up_bf = w_up.astype(jnp.bfloat16)
    down_bf = w_down.astype(jnp.bfloat16)
    partial_value = jnp.dot(normed, up_bf, preferred_element_type=jnp.float32)
    preact = lax.psum(partial_value, "ra")
    activated = jnp.square(jax.nn.relu(preact)).astype(jnp.bfloat16)
    down_part = jnp.dot(activated, down_bf, preferred_element_type=jnp.float32)
    branch = lax.psum(down_part.astype(jnp.bfloat16), "cb").astype(jnp.float32)
    return (RESIDUAL * floated + branch).astype(jnp.bfloat16)


def local(stream, gain_first, up_first, down_first, gain_second, up_second, down_second):
    middle = sublayer(stream, gain_first, up_first, down_first)
    return sublayer(middle, gain_second, up_second, down_second)


def solution(mesh):
    return jax.shard_map(
        local,
        mesh=mesh,
        in_specs=(
            P(None, "ra"),
            P("ra"),
            P("ra", "cb"),
            P("cb", "ra"),
            P("ra"),
            P("ra", "cb"),
            P("cb", "ra"),
        ),
        out_specs=P(None, "ra"),
        check_vma=False,
    )
```

profile of v0, /device:TPU:0, one launch (start us, length us, event | category | flops | bytes accessed | tf_op | source)
XLA Modules:
  0.0 221.5 jit_solution(7013383935762173612)
XLA Ops:
  6.5 0.0 copy-start.3
  6.5 0.0 all-reduce.3.cloned.1.call-start
  6.5 0.9 fusion.10
  7.4 23.2 %psum.42 = f32[64,1]{0,1:T(1,128)S(1)} all-reduce(f32[64,1]{0,1:T(1,128)S(1)} %bitcast.7), channel_id=1, replica_groups=mesh['ra'=8,'cb'=4] {'ra'}, use_global_device_ids=true, to_apply=%region_1.0 | all-reduce | flops 64 | bytes 512 | tf_op jit(solution)/shard_map/psum | solution.py:14
  30.6 0.0 copy-start.4
  30.6 0.0 copy-done.3
  30.6 0.6 copy-done.4
  31.2 0.0 copy-start.1
  31.2 2.0 fusion.4
  33.3 0.0 copy-start
  33.3 0.0 all-reduce.3.cloned.1.call-update
  33.3 0.0 all-reduce.5.cloned.1.call-start
  33.4 68.4 %all-reduce.3.cloned.1.call-done = f32[64,1024]{1,0:T(8,128)} async-done(((f32[64,1024]{1,0:T(8,128)}), f32[64,1024]{1,0:T(8,128)}) %all-reduce.3.cloned.1.call-update) | async-done | bytes 262160 | tf_op jit(solution)/shard_map/psum | solution.py:20
  101.7 0.0 copy-done.1
  101.7 1.1 convolution_convert_fusion.1
  102.8 10.1 %psum.44 = bf16[64,128]{1,0:T(8,128)(2,1)S(1)} all-reduce(bf16[64,128]{1,0:T(8,128)(2,1)S(1)} %convolution_convert_fusion.1), channel_id=1, replica_groups=mesh['ra'=8,'cb'=4] {'cb'}, use_global_device_ids=true, to_apply=%region_3.4 | all-reduce | flops 8192 | bytes 32768 | tf_op jit(solution)/shard_map/psum | solution.py:23
  113.0 0.1 fusion.15
  113.1 19.6 %psum.45 = f32[64,1]{0,1:T(1,128)S(1)} all-reduce(f32[64,1]{0,1:T(1,128)S(1)} %bitcast.6), channel_id=1, replica_groups=mesh['ra'=8,'cb'=4] {'ra'}, use_global_device_ids=true, to_apply=%region_5.6 | all-reduce | flops 64 | bytes 512 | tf_op jit(solution)/shard_map/psum | solution.py:14
  132.7 0.0 copy-start.5
  132.7 0.0 copy-done
  132.7 0.6 copy-done.5
  133.3 0.0 copy-start.2
  133.3 0.9 fusion.1
  134.3 0.0 all-reduce.5.cloned.1.call-update
  134.3 68.5 %all-reduce.5.cloned.1.call-done = f32[64,1024]{1,0:T(8,128)} async-done(((f32[64,1024]{1,0:T(8,128)}), f32[64,1024]{1,0:T(8,128)}) %all-reduce.5.cloned.1.call-update) | async-done | bytes 262160 | tf_op jit(solution)/shard_map/psum | solution.py:20
  202.8 0.0 copy-done.2
  202.8 1.1 convolution_convert_fusion
  203.9 10.1 %psum.47 = bf16[64,128]{1,0:T(8,128)(2,1)S(1)} all-reduce(bf16[64,128]{1,0:T(8,128)(2,1)S(1)} %convolution_convert_fusion), channel_id=1, replica_groups=mesh['ra'=8,'cb'=4] {'cb'}, use_global_device_ids=true, to_apply=%region_7.8 | all-reduce | flops 8192 | bytes 32768 | tf_op jit(solution)/shard_map/psum | solution.py:23
  214.1 0.6 fusion.14
  (2 shorter events, 0.0 us)
Async XLA Ops:
  6.5 24.1 %copy-start.3 = (bf16[64,128]{1,0:T(8,128)(2,1)S(1)}, bf16[64,128]{1,0:T(8,128)(2,1)}, u32[]{:S(2)}) copy-start(bf16[64,128]{1,0:T(8,128)(2,1)} %param.7) | copy-start | bytes 49156
  6.5 95.2 %all-reduce.3.cloned.1.call-start = ((), (), s32[]{:S(2)}) async-start(), calls=%async_computation | async-start | bytes 524288 | tf_op jit(solution)/shard_map/psum | solution.py:20
  30.6 0.7 copy-start.4
  31.2 70.5 %copy-start.1 = (f32[1024,128]{1,0:T(8,128)S(1)}, f32[1024,128]{1,0:T(8,128)}, u32[]{:S(2)}) copy-start(f32[1024,128]{1,0:T(8,128)} %param.10) | copy-start | bytes 1572868
  33.3 99.4 %copy-start = (f32[128,1024]{1,0:T(8,128)S(1)}, f32[128,1024]{1,0:T(8,128)}, u32[]{:S(2)}) copy-start(f32[128,1024]{1,0:T(8,128)} %param.12) | copy-start | bytes 1572868
  33.3 169.5 %all-reduce.5.cloned.1.call-start = ((), (), s32[]{:S(2)}) async-start(), calls=%async_computation.1 | async-start | bytes 524288 | tf_op jit(solution)/shard_map/psum | solution.py:20
  132.7 0.7 copy-start.5
  133.3 69.5 %copy-start.2 = (f32[1024,128]{1,0:T(8,128)S(1)}, f32[1024,128]{1,0:T(8,128)}, u32[]{:S(2)}) copy-start(f32[1024,128]{1,0:T(8,128)} %param.13) | copy-start | bytes 1572868
Sparse Core Ops, SparseCore 0:
  33.4 68.2 all-reduce.2
  134.4 68.3 all-reduce.4
where the time goes:
time: 222 us
  waiting for transfers between devices  137 us (62%)
  blocking collectives  63 us (28%)
  between operations  13.4 us (6%)
  matrix products  5.2 us (2%)
    psum x2, waiting for transfers between devices, sublayer(): preact = lax.psum(partial_value, 'ra')  137 us
    psum x2, blocking collectives, sublayer(): squares = lax.psum(own_squares, 'ra')  42.8 us
    psum x2, blocking collectives, sublayer(): branch = lax.psum(down_part.astype(jnp.bfloat16), 'cb').astype(jnp.float32)  20.2 us
  transfers between devices with their start and end apart: 2, of which 2 were waited for; matrix products, arithmetic and copies ran while one was open for 0% of the time, Pallas kernels for 0%

commit v1 on v0

--- a/solution.py
+++ b/solution.py
@@ -6,6 +6,12 @@
 D = 1024
 EPS = 1e-06
 RESIDUAL = 0.25
+
+
+def summed_here(x, axis):
+    terms = lax.all_gather(x, axis, axis=0, tiled=False)
+    summed = terms.sum(axis=0)
+    return summed
 
 
 def sublayer(stream, norm_gain, w_up, w_down):
@@ -20,7 +26,7 @@
     preact = lax.psum(partial_value, "ra")
     activated = jnp.square(jax.nn.relu(preact)).astype(jnp.bfloat16)
     down_part = jnp.dot(activated, down_bf, preferred_element_type=jnp.float32)
-    branch = lax.psum(down_part.astype(jnp.bfloat16), "cb").astype(jnp.float32)
+    branch = summed_here(down_part.astype(jnp.bfloat16), "cb").astype(jnp.float32)
     return (RESIDUAL * floated + branch).astype(jnp.bfloat16)
 
 

time: 222 us -> 212 us (0.955)
  blocking collectives: 63 us -> 53.2 us
    psum x2 -> x0, blocking collectives: 20.2 us -> none  [sublayer(): branch = lax.psum(down_part.astype(jnp.bfloat16), 'cb').astype(jnp.float32)]
    all_gather x0 -> x2, blocking collectives: none -> 10.5 us  [summed_here(): terms = lax.all_gather(x, axis, axis=0, tiled=False)]
where the time goes in v1:
time: 212 us
  waiting for transfers between devices  137 us (65%)
  blocking collectives  53.2 us (25%)
  between operations  13.5 us (6%)
  matrix products  5.2 us (2%)
    psum x2, waiting for transfers between devices, sublayer(): preact = lax.psum(partial_value, 'ra')  137 us
    psum x2, blocking collectives, sublayer(): squares = lax.psum(own_squares, 'ra')  42.8 us
    all_gather x2, blocking collectives, summed_here(): terms = lax.all_gather(x, axis, axis=0, tiled=False)  10.5 us
  transfers between devices with their start and end apart: 2, of which 2 were waited for; matrix products, arithmetic and copies ran while one was open for 0% of the time, Pallas kernels for 0%

profile of v1, /device:TPU:0, one launch (start us, length us, event | category | flops | bytes accessed | tf_op | source)
XLA Modules:
  0.0 211.6 jit_solution(10804062702338490355)
XLA Ops:
  6.5 0.0 copy-start.3
  6.5 0.0 all-reduce.3.cloned.1.call-start
  6.5 0.9 fusion.10
  7.4 23.2 %psum.28 = f32[64,1]{0,1:T(1,128)S(1)} all-reduce(f32[64,1]{0,1:T(1,128)S(1)} %bitcast.11), channel_id=1, replica_groups=mesh['ra'=8,'cb'=4] {'ra'}, use_global_device_ids=true, to_apply=%region_1.0 | all-reduce | flops 64 | bytes 512 | tf_op jit(solution)/shard_map/psum | solution.py:20
  30.6 0.0 copy-start.4
  30.6 0.0 copy-done.3
  30.6 0.6 copy-done.4
  31.2 0.0 copy-start.1
  31.2 2.0 fusion.4
  33.3 0.0 all-reduce.3.cloned.1.call-update
  33.3 0.0 copy-start
  33.3 0.0 all-reduce.5.cloned.1.call-start
  33.4 68.3 %all-reduce.3.cloned.1.call-done = f32[64,1024]{1,0:T(8,128)} async-done(((f32[64,1024]{1,0:T(8,128)}), f32[64,1024]{1,0:T(8,128)}) %all-reduce.3.cloned.1.call-update) | async-done | bytes 262160 | tf_op jit(solution)/shard_map/psum | solution.py:26
  101.7 0.0 copy-done.1
  101.7 1.1 convolution_convert_fusion.1
  102.8 5.2 %all-gather = bf16[256,128]{1,0:T(8,128)(2,1)S(1)} all-gather(bf16[64,128]{1,0:T(8,128)(2,1)S(1)} %convolution_convert_fusion.1), channel_id=2, replica_groups=mesh['ra'=8,'cb'=4] {'cb'}, dimensions={0}, use_global_device_ids=true | all-gather | bytes 81920 | tf_op jit(solution)/shard_map/all_gather | solution.py:12
  108.1 0.1 fusion.15
  108.2 19.6 %psum.30 = f32[64,1]{0,1:T(1,128)S(1)} all-reduce(f32[64,1]{0,1:T(1,128)S(1)} %bitcast.10), channel_id=1, replica_groups=mesh['ra'=8,'cb'=4] {'ra'}, use_global_device_ids=true, to_apply=%region_5.6 | all-reduce | flops 64 | bytes 512 | tf_op jit(solution)/shard_map/psum | solution.py:20
  127.8 0.0 copy-start.5
  127.8 0.0 copy-done
  127.8 0.6 copy-done.5
  128.5 0.0 copy-start.2
  128.5 0.9 fusion.1
  129.4 0.0 all-reduce.5.cloned.1.call-update
  129.4 68.4 %all-reduce.5.cloned.1.call-done = f32[64,1024]{1,0:T(8,128)} async-done(((f32[64,1024]{1,0:T(8,128)}), f32[64,1024]{1,0:T(8,128)}) %all-reduce.5.cloned.1.call-update) | async-done | bytes 262160 | tf_op jit(solution)/shard_map/psum | solution.py:26
  197.8 0.0 copy-done.2
  197.8 1.1 convolution_convert_fusion
  198.9 5.2 %all-gather.1 = bf16[256,128]{1,0:T(8,128)(2,1)S(1)} all-gather(bf16[64,128]{1,0:T(8,128)(2,1)S(1)} %convolution_convert_fusion), channel_id=3, replica_groups=mesh['ra'=8,'cb'=4] {'cb'}, dimensions={0}, use_global_device_ids=true | all-gather | bytes 81920 | tf_op jit(solution)/shard_map/all_gather | solution.py:12
  204.2 0.6 fusion.14
  (4 shorter events, 0.0 us)
Async XLA Ops:
  6.5 24.1 %copy-start.3 = (bf16[64,128]{1,0:T(8,128)(2,1)S(1)}, bf16[64,128]{1,0:T(8,128)(2,1)}, u32[]{:S(2)}) copy-start(bf16[64,128]{1,0:T(8,128)(2,1)} %param.7) | copy-start | bytes 49156
  6.5 95.2 %all-reduce.3.cloned.1.call-start = ((), (), s32[]{:S(2)}) async-start(), calls=%async_computation | async-start | bytes 524288 | tf_op jit(solution)/shard_map/psum | solution.py:26
  30.6 0.7 copy-start.4
  31.2 70.5 %copy-start.1 = (f32[1024,128]{1,0:T(8,128)S(1)}, f32[1024,128]{1,0:T(8,128)}, u32[]{:S(2)}) copy-start(f32[1024,128]{1,0:T(8,128)} %param.10) | copy-start | bytes 1572868
  33.3 94.5 %copy-start = (f32[128,1024]{1,0:T(8,128)S(1)}, f32[128,1024]{1,0:T(8,128)}, u32[]{:S(2)}) copy-start(f32[128,1024]{1,0:T(8,128)} %param.12) | copy-start | bytes 1572868
  33.3 164.5 %all-reduce.5.cloned.1.call-start = ((), (), s32[]{:S(2)}) async-start(), calls=%async_computation.1 | async-start | bytes 524288 | tf_op jit(solution)/shard_map/psum | solution.py:26
  127.8 0.7 copy-start.5
  128.5 69.3 %copy-start.2 = (f32[1024,128]{1,0:T(8,128)S(1)}, f32[1024,128]{1,0:T(8,128)}, u32[]{:S(2)}) copy-start(f32[1024,128]{1,0:T(8,128)} %param.13) | copy-start | bytes 1572868
Sparse Core Ops, SparseCore 0:
  33.4 68.2 all-reduce.2
  129.5 68.2 all-reduce.4
